TPU v7x, 32 devices: a whole 2x2x4 slice. The times are simulated.
32 devices in a mesh: ep: 8 (over z, x), tp: 4 (over y, core).
Axes of the slice: x: 2, y: 2, z: 4, core: 2. Of those that a mesh axis runs over, the one named last changes fastest.
Arguments:
- hidden_in: bfloat16 [128, 1024], P('ep'), may hold values from -6 to 6
- attn_gain: float32 [1024], replicated, may hold values from 0.1 to 1.9
- w_qdown: bfloat16 [1024, 256], replicated, may hold values from -0.1875 to 0.1875
- q_gain: float32 [256], replicated, may hold values from 0.1 to 1.9
- w_qnope: bfloat16 [256, 512], replicated, may hold values from -0.375 to 0.375
- w_qrope: bfloat16 [256, 256], replicated, may hold values from -0.375 to 0.375
- w_kvdown: bfloat16 [1024, 128], replicated, may hold values from -0.1875 to 0.1875
- kv_gain: float32 [128], replicated, may hold values from 0.1 to 1.9
- w_krope: bfloat16 [1024, 32], replicated, may hold values from -0.1875 to 0.1875
- w_ukey: bfloat16 [128, 512], replicated, may hold values from -0.75 to 0.75
- w_uvalue: bfloat16 [128, 512], replicated, may hold values from -0.5 to 0.5
- w_out: bfloat16 [512, 1024], P('tp'), may hold values from -0.25 to 0.25
- cache_latent: bfloat16 [128, 1024, 128], P(('ep', 'tp')), may hold values from -6 to 6
- cache_rope: bfloat16 [128, 32, 1024], P(('ep', 'tp')), may hold values from -900 to 900
- lengths: int32 [128], P(('ep', 'tp')), may hold values from 1 to 1024, as said below
- ffn_gain: float32 [1024], replicated, may hold values from 0.1 to 1.9
- routes: int32 [128, 2], P('ep'), may hold values from 0 to 3, all different within a row; in each aligned block of 16 rows (0 to 15, 16 to 31, ...) at most 16 rows name the same one
- route_weights: float32 [128, 2], P('ep'), may hold values from 0.25 to 1
- w_gate: bfloat16 [8, 1024, 1792], P('ep', None, 'tp'), may hold values from -0.1875 to 0.1875
- w_up: bfloat16 [8, 1024, 1792], P('ep', None, 'tp'), may hold values from -0.1875 to 0.1875
- w_down: bfloat16 [8, 1792, 1024], P('ep', 'tp'), may hold values from -0.09375 to 0.09375
Outputs:
- next_hidden: bfloat16 [128, 1024], P('ep', 'tp')
Inputs may be any that keep to these rules, and one draw needn't show every extreme that they name: `lengths`: each sequence has 1 to 1024 valid cached positions; in every aligned block of 16 sequences one has all 1024. `routes`: each row names two different experts. In the aligned blocks of 16 rows no expert is named by more than 16 rows, and in some block one expert is named by exactly 16.
All inputs are finite; a program needn't handle non-finite values.
Results may differ from a plain program's by a relative error of at most 0.014.
The roundings to bfloat16 on the way count: a program that leaves them out, or rounds other values in their place, can miss the bound.
Values may be sent and summed in bfloat16 or wider, within the bound.
A program may use at most 64 MiB of HBM per device.

v0:
```python
import jax
import jax.numpy as jnp
from jax import lax
from jax.sharding import PartitionSpec as P

HEADS = 8
NOPE = 64
ROPE = 32
VDIM = 64
KVLORA = 128
eps = 1e-06
rope_base = 10000.0


def rms_scale(values, gain):
    return values * lax.rsqrt(jnp.mean(values * values, axis=-1, keepdims=True) + eps) * gain


def rotate(values, positions):
    width = values.shape[-1]
    middle = width // 2
    inverse = jnp.power(rope_base, -jnp.arange(0, width, 2).astype(jnp.float32) / width)
    angles = positions.astype(jnp.float32)[:, None] * inverse[None, :]
    angles = jnp.concatenate([angles, angles], axis=-1)
    target = (angles.shape[0],) + (1,) * (values.ndim - 2) + (width,)
    cosine = jnp.cos(angles).reshape(target)
    sine = jnp.sin(angles).reshape(target)
    turned = jnp.concatenate([-values[..., middle:], values[..., :middle]], axis=-1)
    return values * cosine + turned * sine


def route_slots(route_table, expert_count):
    flat_ids = route_table.reshape(-1)
    onehot = (flat_ids[:, None] == jnp.arange(expert_count, dtype=jnp.int32)[None, :]).astype(
        jnp.int32
    )
    before = jnp.cumsum(onehot, axis=0) - onehot
    return jnp.sum(before * onehot, axis=1).reshape(route_table.shape)


def unit_block(arrived, w_gate, w_up, w_down):
    gate_part = jnp.einsum("scd,df->scf", arrived, w_gate[0], preferred_element_type=jnp.float32)
    up_part = jnp.einsum("scd,df->scf", arrived, w_up[0], preferred_element_type=jnp.float32)
    inner = (jax.nn.silu(gate_part) * up_part).astype(jnp.bfloat16)
    block_term = jnp.einsum("scf,fd->scd", inner, w_down[0], preferred_element_type=jnp.float32)
    summed = lax.psum_scatter(
        block_term.astype(jnp.bfloat16), "tp", scatter_dimension=2, tiled=True
    )
    return lax.all_to_all(summed, "ep", split_axis=0, concat_axis=0, tiled=True)


def per_device(
    hidden_in,
    attn_gain,
    w_qdown,
    q_gain,
    w_qnope,
    w_qrope,
    w_kvdown,
    kv_gain,
    w_krope,
    w_ukey,
    w_uvalue,
    w_out,
    cache_latent,
    cache_rope,
    lengths,
    ffn_gain,
    routes,
    route_weights,
    w_gate,
    w_up,
    w_down,
):
    group_rows, width = hidden_in.shape
    own_count = lengths.shape[0]
    tp_rank = lax.axis_index("tp")
    score_scale = (NOPE + ROPE) ** (-0.5)
    own_rows = lax.dynamic_slice_in_dim(hidden_in, tp_rank * own_count, own_count, 0).astype(
        jnp.float32
    )
    normed = rms_scale(own_rows, attn_gain).astype(jnp.bfloat16)
    q_small = rms_scale(
        jnp.dot(normed, w_qdown, preferred_element_type=jnp.float32), q_gain
    ).astype(jnp.bfloat16)
    q_plain = (
        jnp.dot(q_small, w_qnope, preferred_element_type=jnp.float32)
        .astype(jnp.bfloat16)
        .reshape(own_count, HEADS, NOPE)
    )
    q_turned = rotate(
        jnp.dot(q_small, w_qrope, preferred_element_type=jnp.float32).reshape(
            own_count, HEADS, ROPE
        ),
        lengths,
    ).astype(jnp.bfloat16)
    q_latent = jnp.einsum(
        "shn,chn->shc",
        q_plain,
        w_ukey.reshape(KVLORA, HEADS, NOPE),
        preferred_element_type=jnp.float32,
    ).astype(jnp.bfloat16)
    new_latent = rms_scale(
        jnp.dot(normed, w_kvdown, preferred_element_type=jnp.float32), kv_gain
    ).astype(jnp.bfloat16)
    new_rope = rotate(jnp.dot(normed, w_krope, preferred_element_type=jnp.float32), lengths).astype(
        jnp.bfloat16
    )
    past_scores = (
        jnp.einsum("shc,spc->shp", q_latent, cache_latent, preferred_element_type=jnp.float32)
        + jnp.einsum("shr,srp->shp", q_turned, cache_rope, preferred_element_type=jnp.float32)
    ) * score_scale
    in_range = jnp.arange(cache_latent.shape[1])[None, None, :] < lengths[:, None, None]
    past_scores = jnp.where(in_range, past_scores, -1e30)
    fresh_score = (
        jnp.einsum("shc,sc->sh", q_latent, new_latent, preferred_element_type=jnp.float32)
        + jnp.einsum("shr,sr->sh", q_turned, new_rope, preferred_element_type=jnp.float32)
    ) * score_scale
    highest = jnp.maximum(jnp.max(past_scores, axis=-1), fresh_score)
    past_exp = jnp.exp(past_scores - highest[..., None])
    fresh_exp = jnp.exp(fresh_score - highest)
    divisor = jnp.sum(past_exp, axis=-1) + fresh_exp
    past_prob = (past_exp / divisor[..., None]).astype(jnp.bfloat16)
    fresh_prob = (fresh_exp / divisor).astype(jnp.bfloat16)
    latent_mix = (
        jnp.einsum("shp,spc->shc", past_prob, cache_latent, preferred_element_type=jnp.float32)
        + fresh_prob.astype(jnp.float32)[..., None] * new_latent.astype(jnp.float32)[:, None, :]
    ).astype(jnp.bfloat16)
    head_values = (
        jnp.einsum(
            "shc,chv->shv",
            latent_mix,
            w_uvalue.reshape(KVLORA, HEADS, VDIM),
            preferred_element_type=jnp.float32,
        )
        .astype(jnp.bfloat16)
        .reshape(own_count, HEADS * VDIM)
    )
    by_heads = lax.all_to_all(head_values, "tp", split_axis=1, concat_axis=0, tiled=True)
    attended = lax.psum(
        jnp.dot(by_heads, w_out, preferred_element_type=jnp.float32).astype(jnp.bfloat16), "tp"
    ).astype(jnp.float32)
    residual = hidden_in.astype(jnp.float32) + attended
    normed_two = rms_scale(residual, ffn_gain).astype(jnp.bfloat16)
    unit_count = lax.axis_size("ep")
    expert_count = unit_count // 2
    capacity = max(2, 4 * group_rows // expert_count)
    quarter = width // lax.axis_size("tp")
    slots = route_slots(routes, expert_count)
    expert_of_unit = jnp.arange(unit_count, dtype=jnp.int32) // 2
    slot_range = jnp.arange(capacity, dtype=jnp.int32)
    chosen = (routes[None, None, :, :] == expert_of_unit[:, None, None, None]) & (
        slots[None, None, :, :] == slot_range[None, :, None, None]
    )
    chooser = jnp.sum(chosen.astype(jnp.int32), axis=-1).astype(jnp.bfloat16)
    outgoing = jnp.einsum(
        "ucr,rd->ucd", chooser, normed_two, preferred_element_type=jnp.float32
    ).astype(jnp.bfloat16)
    returned = unit_block(
        lax.all_to_all(outgoing, "ep", split_axis=0, concat_axis=0, tiled=True),
        w_gate,
        w_up,
        w_down,
    )
    stacked = returned.reshape(unit_count * capacity, quarter)
    first_row = routes * (2 * capacity) + slots
    first_half = stacked[first_row].astype(jnp.float32)
    second_half = stacked[first_row + capacity].astype(jnp.float32)
    blended = jnp.sum(route_weights[..., None] * (first_half + second_half), axis=1)
    own_columns = lax.dynamic_slice_in_dim(residual, tp_rank * quarter, quarter, 1)
    return (own_columns + blended).astype(jnp.bfloat16)


def solution(mesh):
    placed = (
        P("ep", None),
        P(),
        P(),
        P(),
        P(),
        P(),
        P(),
        P(),
        P(),
        P(),
        P(),
        P("tp", None),
        P(("ep", "tp"), None, None),
        P(("ep", "tp"), None, None),
        P(("ep", "tp")),
        P(),
        P("ep", None),
        P("ep", None),
        P("ep", None, "tp"),
        P("ep", None, "tp"),
        P("ep", "tp", None),
    )
    return jax.shard_map(
        per_device, mesh=mesh, in_specs=placed, out_specs=P("ep", "tp"), check_vma=False
    )
```

profile of v0, /device:TPU:0, one launch (start us, length us, event | category | flops | bytes accessed | tf_op | source)
XLA Modules:
  0.0 95.3 jit_solution(16051706030308229401)
XLA Ops:
  6.5 0.8 convert_element_type.106
  7.3 0.7 iota_compare_fusion.2
  8.0 0.8 fusion.25
  8.9 1.1 %fusion.49 = f32[4,32]{1,0:T(4,128)S(1)} fusion(bf16[1024,32]{0,1:T(8,128)(2,1)} %param.29, f32[1024]{0:T(1024)} %param.22, f32[4]{0:T(128)S(1)} %add_rsqrt_fusion.3, bf16[16,1024]{1,0:T(8,128)(2,1)S(1)} %copy-done.4, s32[]{:T(128)S(6)} %select_n.25), kind=kOutput, calls=%fused_computation.101 | convolution fusion | flops 278528 | bytes 78852 | tf_op jit(solution)/shard_map/dot_general | solution.py:106
  10.0 1.4 %multiply_reduce_fusion.2 = (f32[4]{0:T(128)S(1)}, f32[4,256]{1,0:T(4,128)S(1)}) fusion(bf16[1024,256]{1,0:T(8,128)(2,1)} %param.23, f32[1024]{0:T(1024)S(1)} %copy-done.8, f32[4]{0:T(128)S(1)} %add_rsqrt_fusion.3, bf16[16,1024]{1,0:T(8,128)(2,1)S(1)} %copy-done.4, s32[]{:T(128)S(6)} %select_n.25), kind=kOutput, calls=%fused_computation.66 | convolution fusion | flops 2115580 | bytes 541204 | tf_op jit(solution)/shard_map/dot_general | solution.py:84
  11.4 0.7 copy-done.16
  12.7 0.6 copy-done.5
  14.8 0.7 copy-done.11
  15.7 0.5 fusion.56
  16.3 0.7 copy-done.6
  17.8 0.6 copy.74
  18.4 4.3 %all-to-all-start = ((bf16[4,4,128]{2,0,1:T(4,128)(2,1)}), bf16[4,4,128]{2,0,1:T(4,128)(2,1)S(1)}, u32[]{:S(2)}, u32[]{:S(2)}) async-start(bf16[4,4,128]{2,0,1:T(4,128)(2,1)} %copy.74), calls=%async_computation | async-start | bytes 8192 | tf_op jit(solution)/shard_map/all_to_all | solution.py:139
  23.5 3.0 %all-to-all-done = bf16[4,4,128]{2,0,1:T(4,128)(2,1)S(1)} async-done(((bf16[4,4,128]{2,0,1:T(4,128)(2,1)}), bf16[4,4,128]{2,0,1:T(4,128)(2,1)S(1)}, u32[]{:S(2)}, u32[]{:S(2)}) %all-to-all-start) | async-done | bytes 4128 | tf_op jit(solution)/shard_map/all_to_all | solution.py:139
  26.6 10.3 %psum.7 = bf16[16,1024]{1,0:T(8,128)(2,1)S(1)} all-reduce(bf16[16,1024]{1,0:T(8,128)(2,1)S(1)} %convolution_convert_fusion.2), channel_id=1, replica_groups=mesh['ep'=8,'tp'=4] {'tp'}, use_global_device_ids=true, to_apply=%region_5.6 | all-reduce | flops 16384 | bytes 65536 | tf_op jit(solution)/shard_map/psum | solution.py:140
  37.3 15.4 %all_to_all.29 = bf16[8,16,1024]{2,1,0:T(8,128)(2,1)S(1)} all-to-all(bf16[8,16,1024]{2,1,0:T(8,128)(2,1)S(1)} %convolution_convert_fusion), channel_id=1, replica_groups=mesh['ep'=8,'tp'=4] {'ep'}, dimensions={0} | all-to-all | bytes 524288 | tf_op jit(solution)/shard_map/all_to_all | solution.py:160
  52.7 0.4 fusion.9
  53.1 2.6 %convolution_convert_fusion.1 = bf16[8,16,1024]{2,1,0:T(8,128)(2,1)} fusion(bf16[8,16,1024]{2,1,0:T(8,128)(2,1)S(1)} %all_to_all.29, bf16[1,448,1024]{2,1,0:T(8,128)(2,1)S(1)} %copy-done.12, bf16[1,1024,448]{1,2,0:T(8,128)(2,1)} %param.40, f32[8,16,448]{2,1,0:T(8,128)S(1)} %fusion.9), kind=kOutput, calls=%fused_computation.3 | convolution fusion | flops 235356160 | bytes 2588672 | tf_op jit(solution)/shard_map/scf,fd->scd/dot_general | solution.py:45
  55.9 18.1 %reduce-scatter.2.cloned.1.call-done = bf16[8,16,256]{2,1,0:T(8,128)(2,1)} async-done(((bf16[8,16,1024]{2,1,0:T(8,128)(2,1)}), bf16[8,16,256]{2,1,0:T(8,128)(2,1)}) %reduce-scatter.2.cloned.1.call-update) | async-done | bytes 65552 | tf_op jit(solution)/shard_map/reduce_scatter | solution.py:46
  74.0 5.5 %all-to-all-start.2 = ((bf16[8,16,256]{2,1,0:T(8,128)(2,1)}), bf16[8,16,256]{2,1,0:T(8,128)(2,1)S(1)}, u32[]{:S(2)}, u32[]{:S(2)}) async-start(bf16[8,16,256]{2,1,0:T(8,128)(2,1)} %reduce-scatter.2.cloned.1.call-done), calls=%async_computation.3 | async-start | bytes 131072 | tf_op jit(solution)/shard_map/all_to_all | solution.py:49
  79.7 0.6 copy-done.10
  80.4 6.0 %all-to-all-done.2 = bf16[8,16,256]{2,1,0:T(8,128)(2,1)S(1)} async-done(((bf16[8,16,256]{2,1,0:T(8,128)(2,1)}), bf16[8,16,256]{2,1,0:T(8,128)(2,1)S(1)}, u32[]{:S(2)}, u32[]{:S(2)}) %all-to-all-start.2) | async-done | bytes 65568 | tf_op jit(solution)/shard_map/all_to_all | solution.py:49
  86.4 0.6 gather_fusion
  87.1 0.6 gather_fusion.1
  87.8 0.6 add_convert_fusion
  (84 shorter events, 5.2 us)
Async XLA Ops:
  6.5 9.1 %copy-start = (bf16[4,1024,128]{2,1,0:T(8,128)(2,1)S(1)}, bf16[4,1024,128]{2,1,0:T(8,128)(2,1)}, u32[]{:S(2)}) copy-start(bf16[4,1024,128]{2,1,0:T(8,128)(2,1)} %param.33) | copy-start | bytes 3145732
  6.5 2.3 %copy-start.4 = (bf16[16,1024]{1,0:T(8,128)(2,1)S(1)}, bf16[16,1024]{1,0:T(8,128)(2,1)}, u32[]{:S(2)}) copy-start(bf16[16,1024]{1,0:T(8,128)(2,1)} %param.21) | copy-start | bytes 98308
  8.9 1.1 %copy-start.8 = (f32[1024]{0:T(1024)S(1)}, f32[1024]{0:T(1024)}, u32[]{:S(2)}) copy-start(f32[1024]{0:T(1024)} %param.22) | copy-start | bytes 12292
  10.0 1.5 %copy-start.15 = (bf16[256,256]{1,0:T(8,128)(2,1)S(1)}, bf16[256,256]{1,0:T(8,128)(2,1)}, u32[]{:S(2)}) copy-start(bf16[256,256]{1,0:T(8,128)(2,1)} %param.26) | copy-start | bytes 393220
  10.0 2.5 %copy-start.13 = (bf16[256,512]{1,0:T(8,128)(2,1)S(1)}, bf16[256,512]{1,0:T(8,128)(2,1)}, u32[]{:S(2)}) copy-start(bf16[256,512]{1,0:T(8,128)(2,1)} %param.25) | copy-start | bytes 786436
  11.4 0.7 copy-start.16
  12.3 0.9 copy-start.5
  12.4 1.3 %copy-start.3 = (bf16[4,32,1024]{2,1,0:T(8,128)(2,1)S(1)}, bf16[4,32,1024]{2,1,0:T(8,128)(2,1)}, u32[]{:S(2)}) copy-start(bf16[4,32,1024]{2,1,0:T(8,128)(2,1)} %param.34) | copy-start | bytes 786436
  13.4 1.0 %copy-start.14 = (bf16[1024,128]{1,0:T(8,128)(2,1)S(1)}, bf16[1024,128]{1,0:T(8,128)(2,1)}, u32[]{:S(2)}) copy-start(bf16[1024,128]{1,0:T(8,128)(2,1)} %param.27) | copy-start | bytes 786436
  14.8 0.7 copy-start.11
  16.1 0.9 copy-start.6
  17.2 5.5 %copy-start.7 = (s32[16,2]{0,1:T(2,128)S(1)}, s32[16,2]{0,1:T(2,128)}, u32[]{:S(2)}) copy-start(s32[16,2]{0,1:T(2,128)} %param.37) | copy-start | bytes 388
  17.2 9.3 %copy-start.2 = (bf16[128,1024]{1,0:T(8,128)(2,1)S(1)}, bf16[128,1024]{1,0:T(8,128)(2,1)}, u32[]{:S(2)}) copy-start(bf16[128,1024]{1,0:T(8,128)(2,1)} %param.32) | copy-start | bytes 786436
  17.2 19.8 %copy-start.9 = (f32[1024]{0:T(1024)S(1)}, f32[1024]{0:T(1024)}, u32[]{:S(2)}) copy-start(f32[1024]{0:T(1024)} %param.36) | copy-start | bytes 12292
  17.5 35.2 %copy-start.1 = (bf16[1,1024,448]{1,2,0:T(8,128)(2,1)S(1)}, bf16[1,1024,448]{1,2,0:T(8,128)(2,1)}, u32[]{:S(2)}) copy-start(bf16[1,1024,448]{1,2,0:T(8,128)(2,1)} %param.39) | copy-start | bytes 2752516
  18.4 8.1 %all-to-all-start = ((bf16[4,4,128]{2,0,1:T(4,128)(2,1)}), bf16[4,4,128]{2,0,1:T(4,128)(2,1)S(1)}, u32[]{:S(2)}, u32[]{:S(2)}) async-start(bf16[4,4,128]{2,0,1:T(4,128)(2,1)} %copy.74), calls=%async_computation | async-start | bytes 8192 | tf_op jit(solution)/shard_map/all_to_all | solution.py:139
  22.7 51.3 %reduce-scatter.2.cloned.1.call-start = ((), (), s32[]{:S(2)}) async-start(), calls=%async_computation.4 | async-start | bytes 327680 | tf_op jit(solution)/shard_map/reduce_scatter | solution.py:46
  37.3 15.8 %copy-start.12 = (bf16[1,448,1024]{2,1,0:T(8,128)(2,1)S(1)}, bf16[1,448,1024]{2,1,0:T(8,128)(2,1)}, u32[]{:S(2)}) copy-start(bf16[1,448,1024]{2,1,0:T(8,128)(2,1)} %param.41) | copy-start | bytes 2752516
  74.0 12.4 %all-to-all-start.2 = ((bf16[8,16,256]{2,1,0:T(8,128)(2,1)}), bf16[8,16,256]{2,1,0:T(8,128)(2,1)S(1)}, u32[]{:S(2)}, u32[]{:S(2)}) async-start(bf16[8,16,256]{2,1,0:T(8,128)(2,1)} %reduce-scatter.2.cloned.1.call-done), calls=%async_computation.3 | async-start | bytes 131072 | tf_op jit(solution)/shard_map/all_to_all | solution.py:49
  79.6 0.7 copy-start.10
Sparse Core Ops, SparseCore 0:
  55.9 18.0 reduce-scatter.1
where the time goes:
time: 95.9 us; the launch traced here: 95.3 us
  waiting for transfers between devices  27.1 us (28%)
  blocking collectives  25.6 us (27%)
  between operations  13.6 us (14%)
  starting transfers between devices  9.79 us (10%)
  matrix products  8.07 us (8%)
  local copies, waits for them, and re-layouts  6.79 us (7%)
  other arithmetic  4.28 us (4%)
    reduce_scatter x1, waiting for transfers between devices, unit_block(): lax.psum_scatter(block_term.astype(jnp.bfloat16), 'tp', scatter_dimension...  18.1 us
    all_to_all x1, blocking collectives, per_device(): lax.all_to_all(outgoing, 'ep', split_axis=0, concat_axis=0, tiled=True)  15.4 us
    psum x1, blocking collectives, per_device(): lax.psum(jnp.dot(by_heads, w_out, preferred_element_type=jnp.float32).ast...  10.3 us
    all_to_all x1, waiting for transfers between devices, unit_block(): return lax.all_to_all(summed, 'ep', split_axis=0, concat_axis=0, tiled=True)  6.04 us
    all_to_all x1, starting transfers between devices, unit_block(): return lax.all_to_all(summed, 'ep', split_axis=0, concat_axis=0, tiled=True)  5.52 us
    all_to_all x1, starting transfers between devices, per_device(): lax.all_to_all(head_values, 'tp', split_axis=1, concat_axis=0, tiled=True)  4.26 us
    unnamed x38, local copies, waits for them, and re-layouts  4.04 us
    all_to_all x1, waiting for transfers between devices, per_device(): lax.all_to_all(head_values, 'tp', split_axis=1, concat_axis=0, tiled=True)  2.99 us
  transfers between devices with their start and end apart: 3, of which 3 were waited for; matrix products, arithmetic and copies ran while one was open for 1% of the time, Pallas kernels for 0%

commit v1 on v0

--- a/solution.py
+++ b/solution.py
@@ -136,7 +136,10 @@
         .astype(jnp.bfloat16)
         .reshape(own_count, HEADS * VDIM)
     )
-    by_heads = lax.all_to_all(head_values, "tp", split_axis=1, concat_axis=0, tiled=True)
+    by_heads = jnp.concatenate(
+        lax.all_to_all(jnp.stack(jnp.split(head_values, lax.axis_size("tp"), axis=1)), "tp", 0, 0),
+        axis=0,
+    )
     attended = lax.psum(
         jnp.dot(by_heads, w_out, preferred_element_type=jnp.float32).astype(jnp.bfloat16), "tp"
     ).astype(jnp.float32)

time: 95.9 us -> 95.9 us (level)
  no operation moved by 1% of the time
where the time goes in v1:
time: 95.9 us; the launch traced here: 95.3 us
  waiting for transfers between devices  27.1 us (28%)
  blocking collectives  25.6 us (27%)
  between operations  13.6 us (14%)
  starting transfers between devices  9.79 us (10%)
  matrix products  8.08 us (8%)
  local copies, waits for them, and re-layouts  6.18 us (6%)
  other arithmetic  4.9 us (5%)
    reduce_scatter x1, waiting for transfers between devices, unit_block(): lax.psum_scatter(block_term.astype(jnp.bfloat16), 'tp', scatter_dimension...  18.1 us
    all_to_all x1, blocking collectives, per_device(): lax.all_to_all(outgoing, 'ep', split_axis=0, concat_axis=0, tiled=True)  15.3 us
    psum x1, blocking collectives, per_device(): lax.psum(jnp.dot(by_heads, w_out, preferred_element_type=jnp.float32).ast...  10.3 us
    all_to_all x1, waiting for transfers between devices, unit_block(): return lax.all_to_all(summed, 'ep', split_axis=0, concat_axis=0, tiled=True)  6.04 us
    all_to_all x1, starting transfers between devices, unit_block(): return lax.all_to_all(summed, 'ep', split_axis=0, concat_axis=0, tiled=True)  5.52 us
    all_to_all x1, starting transfers between devices, per_device(): lax.all_to_all(jnp.stack(jnp.split(head_values, lax.axis_size('tp'), axis...  4.26 us
    unnamed x38, local copies, waits for them, and re-layouts  4.04 us
    all_to_all x1, waiting for transfers between devices, per_device(): lax.all_to_all(jnp.stack(jnp.split(head_values, lax.axis_size('tp'), axis...  2.99 us
  transfers between devices with their start and end apart: 3, of which 3 were waited for; matrix products, arithmetic and copies ran while one was open for 1% of the time, Pallas kernels for 0%

profile of v1, /device:TPU:0, one launch (start us, length us, event | category | flops | bytes accessed | tf_op | source)
XLA Modules:
  0.0 95.3 jit_solution(2506243411484095402)
XLA Ops:
  6.5 0.8 convert_element_type.106
  7.3 0.7 iota_compare_fusion.2
  8.0 0.8 fusion.25
  8.9 1.1 %fusion.49 = f32[4,32]{1,0:T(4,128)S(1)} fusion(bf16[1024,32]{0,1:T(8,128)(2,1)} %param.29, f32[1024]{0:T(1024)} %param.22, f32[4]{0:T(128)S(1)} %add_rsqrt_fusion.3, bf16[16,1024]{1,0:T(8,128)(2,1)S(1)} %copy-done.4, s32[]{:T(128)S(6)} %select_n.25), kind=kOutput, calls=%fused_computation.106 | convolution fusion | flops 278528 | bytes 78852 | tf_op jit(solution)/shard_map/dot_general | solution.py:106
  10.0 1.4 %multiply_reduce_fusion.2 = (f32[4]{0:T(128)S(1)}, f32[4,256]{1,0:T(4,128)S(1)}) fusion(bf16[1024,256]{1,0:T(8,128)(2,1)} %param.23, f32[1024]{0:T(1024)S(1)} %copy-done.8, f32[4]{0:T(128)S(1)} %add_rsqrt_fusion.3, bf16[16,1024]{1,0:T(8,128)(2,1)S(1)} %copy-done.4, s32[]{:T(128)S(6)} %select_n.25), kind=kOutput, calls=%fused_computation.67 | convolution fusion | flops 2115580 | bytes 541204 | tf_op jit(solution)/shard_map/dot_general | solution.py:84
  11.4 0.7 copy-done.16
  12.7 0.6 copy-done.5
  14.8 0.7 copy-done.11
  15.7 0.5 fusion.56
  16.3 0.7 copy-done.6
  17.8 0.6 pad_maximum_fusion
  18.4 4.3 %all-to-all-start = ((bf16[4,4,128]{2,1,0:T(4,128)(2,1)}), bf16[4,4,128]{2,1,0:T(4,128)(2,1)S(1)}, u32[]{:S(2)}, u32[]{:S(2)}) async-start(bf16[4,4,128]{2,1,0:T(4,128)(2,1)} %pad_maximum_fusion), calls=%async_computation | async-start | bytes 8192 | tf_op jit(solution)/shard_map/all_to_all | solution.py:140
  23.5 3.0 %all-to-all-done = bf16[4,4,128]{2,1,0:T(4,128)(2,1)S(1)} async-done(((bf16[4,4,128]{2,1,0:T(4,128)(2,1)}), bf16[4,4,128]{2,1,0:T(4,128)(2,1)S(1)}, u32[]{:S(2)}, u32[]{:S(2)}) %all-to-all-start) | async-done | bytes 4128 | tf_op jit(solution)/shard_map/all_to_all | solution.py:140
  26.6 10.3 %psum.7 = bf16[16,1024]{1,0:T(8,128)(2,1)S(1)} all-reduce(bf16[16,1024]{1,0:T(8,128)(2,1)S(1)} %convolution_convert_fusion.2), channel_id=1, replica_groups=mesh['ep'=8,'tp'=4] {'tp'}, use_global_device_ids=true, to_apply=%region_5.6 | all-reduce | flops 16384 | bytes 65536 | tf_op jit(solution)/shard_map/psum | solution.py:143
  37.3 15.3 %all_to_all.15 = bf16[8,16,1024]{2,1,0:T(8,128)(2,1)S(1)} all-to-all(bf16[8,16,1024]{2,1,0:T(8,128)(2,1)S(1)} %convolution_convert_fusion), channel_id=1, replica_groups=mesh['ep'=8,'tp'=4] {'ep'}, dimensions={0} | all-to-all | bytes 524288 | tf_op jit(solution)/shard_map/all_to_all | solution.py:163
  52.7 0.4 fusion.9
  53.1 2.6 %convolution_convert_fusion.1 = bf16[8,16,1024]{2,1,0:T(8,128)(2,1)} fusion(bf16[8,16,1024]{2,1,0:T(8,128)(2,1)S(1)} %all_to_all.15, bf16[1,448,1024]{2,1,0:T(8,128)(2,1)S(1)} %copy-done.12, bf16[1,1024,448]{1,2,0:T(8,128)(2,1)} %param.40, f32[8,16,448]{2,1,0:T(8,128)S(1)} %fusion.9), kind=kOutput, calls=%fused_computation.3 | convolution fusion | flops 235356160 | bytes 2588672 | tf_op jit(solution)/shard_map/scf,fd->scd/dot_general | solution.py:45
  55.9 18.1 %reduce-scatter.2.cloned.1.call-done = bf16[8,16,256]{2,1,0:T(8,128)(2,1)} async-done(((bf16[8,16,1024]{2,1,0:T(8,128)(2,1)}), bf16[8,16,256]{2,1,0:T(8,128)(2,1)}) %reduce-scatter.2.cloned.1.call-update) | async-done | bytes 65552 | tf_op jit(solution)/shard_map/reduce_scatter | solution.py:46
  74.0 5.5 %all-to-all-start.2 = ((bf16[8,16,256]{2,1,0:T(8,128)(2,1)}), bf16[8,16,256]{2,1,0:T(8,128)(2,1)S(1)}, u32[]{:S(2)}, u32[]{:S(2)}) async-start(bf16[8,16,256]{2,1,0:T(8,128)(2,1)} %reduce-scatter.2.cloned.1.call-done), calls=%async_computation.3 | async-start | bytes 131072 | tf_op jit(solution)/shard_map/all_to_all | solution.py:49
  79.7 0.6 copy-done.10
  80.4 6.0 %all-to-all-done.2 = bf16[8,16,256]{2,1,0:T(8,128)(2,1)S(1)} async-done(((bf16[8,16,256]{2,1,0:T(8,128)(2,1)}), bf16[8,16,256]{2,1,0:T(8,128)(2,1)S(1)}, u32[]{:S(2)}, u32[]{:S(2)}) %all-to-all-start.2) | async-done | bytes 65568 | tf_op jit(solution)/shard_map/all_to_all | solution.py:49
  86.4 0.6 gather_fusion
  87.1 0.6 gather_fusion.1
  87.9 0.6 add_convert_fusion
  (85 shorter events, 5.2 us)
Async XLA Ops:
  6.5 9.1 %copy-start = (bf16[4,1024,128]{2,1,0:T(8,128)(2,1)S(1)}, bf16[4,1024,128]{2,1,0:T(8,128)(2,1)}, u32[]{:S(2)}) copy-start(bf16[4,1024,128]{2,1,0:T(8,128)(2,1)} %param.33) | copy-start | bytes 3145732
  6.5 2.3 %copy-start.4 = (bf16[16,1024]{1,0:T(8,128)(2,1)S(1)}, bf16[16,1024]{1,0:T(8,128)(2,1)}, u32[]{:S(2)}) copy-start(bf16[16,1024]{1,0:T(8,128)(2,1)} %param.21) | copy-start | bytes 98308
  8.9 1.1 %copy-start.8 = (f32[1024]{0:T(1024)S(1)}, f32[1024]{0:T(1024)}, u32[]{:S(2)}) copy-start(f32[1024]{0:T(1024)} %param.22) | copy-start | bytes 12292
  10.0 1.5 %copy-start.15 = (bf16[256,256]{1,0:T(8,128)(2,1)S(1)}, bf16[256,256]{1,0:T(8,128)(2,1)}, u32[]{:S(2)}) copy-start(bf16[256,256]{1,0:T(8,128)(2,1)} %param.26) | copy-start | bytes 393220
  10.0 2.5 %copy-start.13 = (bf16[256,512]{1,0:T(8,128)(2,1)S(1)}, bf16[256,512]{1,0:T(8,128)(2,1)}, u32[]{:S(2)}) copy-start(bf16[256,512]{1,0:T(8,128)(2,1)} %param.25) | copy-start | bytes 786436
  11.4 0.7 copy-start.16
  12.3 0.9 copy-start.5
  12.4 1.3 %copy-start.3 = (bf16[4,32,1024]{2,1,0:T(8,128)(2,1)S(1)}, bf16[4,32,1024]{2,1,0:T(8,128)(2,1)}, u32[]{:S(2)}) copy-start(bf16[4,32,1024]{2,1,0:T(8,128)(2,1)} %param.34) | copy-start | bytes 786436
  13.4 1.0 %copy-start.14 = (bf16[1024,128]{1,0:T(8,128)(2,1)S(1)}, bf16[1024,128]{1,0:T(8,128)(2,1)}, u32[]{:S(2)}) copy-start(bf16[1024,128]{1,0:T(8,128)(2,1)} %param.27) | copy-start | bytes 786436
  14.8 0.7 copy-start.11
  16.1 0.9 copy-start.6
  17.2 5.5 %copy-start.7 = (s32[16,2]{0,1:T(2,128)S(1)}, s32[16,2]{0,1:T(2,128)}, u32[]{:S(2)}) copy-start(s32[16,2]{0,1:T(2,128)} %param.37) | copy-start | bytes 388
  17.2 9.3 %copy-start.2 = (bf16[128,1024]{1,0:T(8,128)(2,1)S(1)}, bf16[128,1024]{1,0:T(8,128)(2,1)}, u32[]{:S(2)}) copy-start(bf16[128,1024]{1,0:T(8,128)(2,1)} %param.32) | copy-start | bytes 786436
  17.2 19.8 %copy-start.9 = (f32[1024]{0:T(1024)S(1)}, f32[1024]{0:T(1024)}, u32[]{:S(2)}) copy-start(f32[1024]{0:T(1024)} %param.36) | copy-start | bytes 12292
  17.5 35.2 %copy-start.1 = (bf16[1,1024,448]{1,2,0:T(8,128)(2,1)S(1)}, bf16[1,1024,448]{1,2,0:T(8,128)(2,1)}, u32[]{:S(2)}) copy-start(bf16[1,1024,448]{1,2,0:T(8,128)(2,1)} %param.39) | copy-start | bytes 2752516
  18.4 8.1 %all-to-all-start = ((bf16[4,4,128]{2,1,0:T(4,128)(2,1)}), bf16[4,4,128]{2,1,0:T(4,128)(2,1)S(1)}, u32[]{:S(2)}, u32[]{:S(2)}) async-start(bf16[4,4,128]{2,1,0:T(4,128)(2,1)} %pad_maximum_fusion), calls=%async_computation | async-start | bytes 8192 | tf_op jit(solution)/shard_map/all_to_all | solution.py:140
  22.7 51.3 %reduce-scatter.2.cloned.1.call-start = ((), (), s32[]{:S(2)}) async-start(), calls=%async_computation.4 | async-start | bytes 327680 | tf_op jit(solution)/shard_map/reduce_scatter | solution.py:46
  37.3 15.8 %copy-start.12 = (bf16[1,448,1024]{2,1,0:T(8,128)(2,1)S(1)}, bf16[1,448,1024]{2,1,0:T(8,128)(2,1)}, u32[]{:S(2)}) copy-start(bf16[1,448,1024]{2,1,0:T(8,128)(2,1)} %param.41) | copy-start | bytes 2752516
  74.0 12.4 %all-to-all-start.2 = ((bf16[8,16,256]{2,1,0:T(8,128)(2,1)}), bf16[8,16,256]{2,1,0:T(8,128)(2,1)S(1)}, u32[]{:S(2)}, u32[]{:S(2)}) async-start(bf16[8,16,256]{2,1,0:T(8,128)(2,1)} %reduce-scatter.2.cloned.1.call-done), calls=%async_computation.3 | async-start | bytes 131072 | tf_op jit(solution)/shard_map/all_to_all | solution.py:49
  79.6 0.7 copy-start.10
Sparse Core Ops, SparseCore 0:
  55.9 18.0 reduce-scatter.1
